TPU v7x, 256 devices: a whole 4x4x8 slice. The times are simulated.
256 devices in a mesh: sp: 32 (over z, y), fs: 4 (over x), tp: 2 (over core).
Axes of the slice: x: 4, y: 4, z: 8, core: 2. Of those that a mesh axis runs over, the one named last changes fastest.
Arguments:
- tokens: bfloat16 [4, 8192, 2048], P('fs', ('sp', 'tp')), may hold values from -6 to 6
- norm_gain: float32 [2048], replicated, may hold values from 0.1 to 1.9
- w_conv_gate: bfloat16 [2048, 1024], P('sp', 'tp'), may hold values from -0.125 to 0.125
- w_conv_in: bfloat16 [2048, 1024], P('sp', 'tp'), may hold values from -0.125 to 0.125
- w_conv_value: bfloat16 [2048, 1024], P('sp', 'tp'), may hold values from -0.125 to 0.125
- conv_taps: float32 [3, 1024], P(None, 'tp'), may hold values from -3.5 to 3.5
- w_receptance: bfloat16 [2048, 1024], P('sp', 'tp'), may hold values from -0.125 to 0.125
- w_key: bfloat16 [2048, 1024], P('sp', 'tp'), may hold values from -0.125 to 0.125
- w_value: bfloat16 [2048, 1024], P('sp', 'tp'), may hold values from -0.125 to 0.125
- w_decay_down: bfloat16 [2048, 128], P('sp'), may hold values from -0.125 to 0.125
- w_decay_up: bfloat16 [128, 1024], P(None, 'tp'), may hold values from -0.75 to 0.75
- decay_base: float32 [1024], P('tp'), may hold values from -12.5 to -3
- decay_shift: float32 [4, 8192, 1024], P('fs', 'sp', 'tp'), may hold values from -2.1 to 0
- w_rate_down: bfloat16 [2048, 128], P('sp'), may hold values from -0.125 to 0.125
- w_rate_up: bfloat16 [128, 1024], P(None, 'tp'), may hold values from -0.5 to 0.5
- rate_base: float32 [1024], P('tp'), may hold values from -10 to 1
- key_scale: float32 [1024], P('tp'), may hold values from 0.25 to 2.5
- key_mix: float32 [1024], P('tp'), may hold values from 0.1 to 0.7
- group_gain: float32 [1024], P('tp'), may hold values from 0.1 to 1.9
- w_out_conv: bfloat16 [1024, 2048], P('tp', 'sp'), may hold values from -0.125 to 0.125
- w_out_state: bfloat16 [1024, 2048], P('tp', 'sp'), may hold values from -0.125 to 0.125
Outputs:
- mixed: bfloat16 [4, 8192, 2048], P('fs', ('sp', 'tp'))
All inputs are finite; a program needn't handle non-finite values.
Results may differ from a plain program's by a relative error of at most 0.015.
Values may be sent and summed in bfloat16 or wider, within the bound.
A program may use at most 128 MiB of HBM per device.

v0:
```python
import jax
import jax.numpy as jnp
from jax import lax
from jax.experimental import pallas as pl
from jax.experimental.pallas import tpu as pltpu
from jax.sharding import Mesh
from jax.sharding import PartitionSpec as P

MESH = pl.DeviceIdType.MESH
AXES = ("sp_0", "sp_1", "fs", "tp")
SP = ("sp_0", "sp_1")
SP_TP = ("sp_0", "sp_1", "tp")
NZ, NY, NX = 8, 4, 4
HEAD = 64
LANES = 128
BLOCK = 64
COLS_IN = 7 * LANES
COLS = 9 * LANES
F32, BF16 = jnp.float32, jnp.bfloat16
norm_eps = 1e-06
group_eps = 0.00064


def here():
    return tuple(lax.axis_index(a) for a in AXES)


def enter(peers):
    barrier = pltpu.get_barrier_semaphore()
    for peer in peers:
        pl.semaphore_signal(barrier, inc=1, device_id=peer, device_id_type=MESH)
    return lambda: pl.semaphore_wait(barrier, len(peers))


def remote(src, dst, send_sem, recv_sem, peer):
    return pltpu.make_async_remote_copy(
        src_ref=src, dst_ref=dst, send_sem=send_sem, recv_sem=recv_sem, device_id=peer, device_id_type=MESH
    )


def gather_kernel(
    tok_ref, gain_ref, wp_ref, shift_ref,
    proj_ref, low_ref, shift_out, wout_ref,
    T, W, DS, LOW,
    w_send, w_recv, a_send, a_recv, s_send, s_recv, t_send, t_recv, c_send, c_recv, l_send, l_recv,
):
    z, y, x, c = here()

    def at(dz=0, dy=0, dx=0, dc=0):
        return (lax.rem(z + dz, NZ), lax.rem(y + dy, NY), lax.rem(x + dx, NX), lax.rem(c + dc, 2))

    peers = [at(dz=1), at(dz=7), at(dx=1), at(dx=3), at(dy=1), at(dy=2), at(dy=3), at(dc=1)]
    entered = enter(peers)
    x16 = pl.multiple_of(x * 16, 16)
    lane_of = lambda yy: pl.ds(pl.multiple_of(yy * LANES, LANES), LANES)
    W[z, y, x] = wp_ref[y, pl.ds(x16, 16), :]
    DS[y] = shift_ref[:, lane_of(y)]
    gain = gain_ref[...]

    @pl.loop(0, 4)
    def _(i):
        rows = pl.ds(pl.multiple_of(i * 32, 32), 32)
        values = tok_ref[rows, :].astype(F32)
        scaled = values * lax.rsqrt(jnp.mean(values * values, axis=-1, keepdims=True) + norm_eps)
        T[y, c, rows, :] = (scaled * gain).astype(BF16)

    entered()
    waits = []

    def go(copy):
        copy.start()
        waits.append(copy)
        return copy

    arrive_a = []
    for d in (1, 3, 2):
        to = lax.rem(y + d, NY)
        arrive_a.append(go(remote(wp_ref.at[to, pl.ds(x16, 16), :], W.at[z, y, x], a_send.at[d - 1], a_recv.at[d - 1], at(dy=d))))
    def token_unit(dy, half):
        return T.at[lax.rem(y + NY - dy, NY), c, pl.ds(half * 64, 64), :]

    def token_send(dy, half, to_dy, via):
        k = to_dy * 2 + half
        return go(remote(token_unit(dy, half), token_unit(dy, half), t_send.at[k], t_recv.at[k], at(dy=via)))

    t10 = token_send(0, 0, 1, 1)
    t31 = token_send(0, 1, 3, 3)
    t11 = token_send(0, 1, 1, 1)
    t30 = token_send(0, 0, 3, 3)
    other = at(dc=1)

    def across(dy):
        unit = T.at[lax.rem(y + NY - dy, NY), c]
        return go(remote(unit, unit, c_send.at[dy], c_recv.at[dy], other))

    crossed = [across(0)]
    for d in (1, 3, 2):
        to = lax.rem(y + d, NY)
        go(remote(shift_ref.at[:, lane_of(to)], DS.at[y], s_send.at[d - 1], s_recv.at[d - 1], at(dy=d)))

    def unit(h, dz, dx):
        return W.at[lax.rem(z + NZ - dz, NZ), pl.ds(2 * h, 2), lax.rem(x + NX - dx, NX)]

    copies = {}

    def send(h, dz, dx, step_z, step_x):
        nz, nx = (dz + step_z) % NZ, (dx + step_x) % NX
        copies[h, nz, nx] = go(
            remote(unit(h, dz, dx), unit(h, dz, dx), w_send.at[h, nz, nx], w_recv.at[h, nz, nx], at(dz=step_z % NZ, dx=step_x % NX))
        )

    def forward(h, dz, dx):
        if h == 0:
            if dx == 0:
                if dz in (0, 1, 2, 3):
                    send(0, dz, 0, 1, 0)
                if dz in (0, 7, 6):
                    send(0, dz, 0, -1, 0)
                send(0, dz, 0, 0, 1)
                send(0, dz, 0, 0, -1)
            elif dx == 1 and dz % 2 == 0:
                send(0, dz, 1, 0, 1)
            elif dx == 3 and dz % 2 == 1:
                send(0, dz, 3, 0, -1)
        else:
            if dz == 0:
                if dx in (0, 1):
                    send(1, 0, dx, 0, 1)
                if dx == 0:
                    send(1, 0, dx, 0, -1)
                send(1, 0, dx, 1, 0)
                send(1, 0, dx, -1, 0)
            elif dz in (1, 2) or (dz == 3 and dx % 2 == 0):
                send(1, dz, dx, 1, 0)
            elif dz in (7, 6) or (dz == 5 and dx % 2 == 1):
                send(1, dz, dx, -1, 0)

    def hops(h, dz, dx):
        return min(dz, NZ - dz) + min(dx, NX - dx)

    for copy in arrive_a:
        copy.wait_recv()
    order = sorted(
        ((h, dz, dx) for h in range(2) for dz in range(NZ) for dx in range(NX)),
        key=lambda u: (hops(*u), u[0], min(u[2], NX - u[2]), u[1]),
    )
    token_at = 12
    for k, u in enumerate(order):
        if k >= 2:
            copies[u].wait_recv()
        forward(*u)
        if k == token_at:
            t10.wait_recv()
            t20 = token_send(1, 0, 2, 1)
            t31.wait_recv()
            t21 = token_send(3, 1, 2, 3)
        if k == token_at + 16:
            t11.wait_recv()
            t30.wait_recv()
            crossed += [across(1), across(3)]
    t20.wait_recv()
    t21.wait_recv()
    crossed.append(across(2))
    for copy in crossed:
        copy.wait_recv()

    def rows_of(i):
        return T[i].reshape(256, 2048)

    @pl.loop(0, NY)
    def _(i):
        w = W[:, :, :, :, 6 * LANES : 7 * LANES].reshape(2048, LANES)
        out = jnp.dot(rows_of(i), w, preferred_element_type=F32)
        LOW[c, pl.ds(pl.multiple_of(i * 256, 256), 256), :] = out.astype(BF16)

    low_copy = remote(LOW.at[c], LOW.at[c], l_send.at[0], l_recv.at[0], other)
    low_copy.start()

    @pl.loop(0, NY)
    def _(i):
        rows = pl.ds(pl.multiple_of(i * 256, 256), 256)
        for n in range(3):
            w = W[:, :, :, :, n * 256 : n * 256 + 256].reshape(2048, 256)
            out = jnp.dot(rows_of(i), w, preferred_element_type=F32)
            proj_ref[rows, n * 256 : n * 256 + 256] = out.astype(BF16)

    wout_ref[...] = W[:, :, :, :, 7 * LANES :].reshape(2048, 256)
    for d in (1, 2, 3):
        to = lax.rem(y + d, NY)
        remote(shift_ref.at[:, lane_of(to)], DS.at[y], s_send.at[d - 1], s_recv.at[d - 1], at(dy=d)).wait_recv()
    shift_out[...] = DS[...].reshape(1024, LANES)
    low_copy.wait_recv()
    low_ref[...] = LOW[...]
    low_copy.wait_send()
    for copy in waits:
        copy.wait_send()


def gather_and_project(tokens, gain, wp, shift):
    vmem = pl.BlockSpec(memory_space=pltpu.VMEM)
    dma = pltpu.SemaphoreType.DMA
    return pl.pallas_call(
        gather_kernel,
        name="gather_project",
        out_shape=(
            jax.ShapeDtypeStruct((1024, 6 * LANES), BF16),
            jax.ShapeDtypeStruct((2, 1024, LANES), BF16),
            jax.ShapeDtypeStruct((1024, LANES), F32),
            jax.ShapeDtypeStruct((2048, 2 * LANES), BF16),
        ),
        in_specs=[vmem] * 4,
        out_specs=(vmem,) * 4,
        scratch_shapes=[
            pltpu.VMEM((NY, 2, 128, 2048), BF16),
            pltpu.VMEM((NZ, NY, NX, 16, COLS), BF16),
            pltpu.VMEM((NY, 256, LANES), F32),
            pltpu.VMEM((2, 1024, LANES), BF16),
            dma((2, NZ, NX)), dma((2, NZ, NX)), dma((3,)), dma((3,)), dma((3,)), dma((3,)),
            dma((8,)), dma((8,)), dma((4,)), dma((4,)), dma((1,)), dma((1,)),
        ],
        compiler_params=pltpu.CompilerParams(collective_id=1, has_side_effects=True, vmem_limit_bytes=48 << 20),
        cost_estimate=pl.CostEstimate(flops=4_000_000_000, bytes_accessed=16_000_000, transcendentals=0),
    )(tokens, gain, wp, shift)


def halves(a):
    high = a.astype(BF16)
    return high, (a - high.astype(F32)).astype(BF16)


def dot(a, b):
    return jnp.dot(a, b, preferred_element_type=F32)


def dot_nt(a, b):
    return lax.dot_general(a, b, (((1,), (1,)), ((), ())), preferred_element_type=F32)


def mm(a, b):
    ah, al = halves(a)
    bh, bl = halves(b)
    both = jnp.concatenate([bh, bl], axis=1)
    out = dot(jnp.concatenate([ah, al], axis=1), jnp.concatenate([both, both], axis=0))
    return out[:, :LANES] + out[:, LANES:]


def mm_wide(a, b):
    ah, al = halves(a)
    bh, bl = halves(b)
    return dot(jnp.concatenate([ah, al], axis=1), jnp.concatenate([bh, bh], axis=0)) + dot(ah, bl)


def mm_nt_wide(a, b):
    ah, al = halves(a)
    bh, bl = halves(b)
    return dot_nt(jnp.concatenate([ah, al], axis=1), jnp.concatenate([bh, bh], axis=1)) + dot_nt(ah, bl)


def head_sum(values, ones):
    high, low = halves(values)
    return dot(high, ones) + dot(low, ones)


def block_kernel(
    y_param, proj_ref, low_ref, shift_ref, up_d_ref, up_r_ref, par_ref,
    qp_ref, loc_ref, gh_ref,
    LD, AD, BD, KW, GC, QM, LO, X,
):
    y = lax.axis_index("sp_1")
    mine = pl.ds(pl.multiple_of(y * LANES, LANES), LANES)
    lane = lax.broadcasted_iota(jnp.int32, (128, LANES), 1)
    row = lax.broadcasted_iota(jnp.int32, (128, LANES), 0)
    same_head = (row // HEAD) == (lane // HEAD)
    ones = jnp.where(same_head, 1.0, 0.0).astype(BF16)
    up_d, up_r = up_d_ref[:, mine], up_r_ref[:, mine]
    decay_base, rate_base = par_ref[0:1, mine], par_ref[1:2, mine]
    key_scale, key_mix = par_ref[2:3, mine], par_ref[3:4, mine]

    @pl.loop(0, 4)
    def _(i):
        rows = pl.ds(pl.multiple_of(i * 256, 256), 256)
        act = jnp.tanh(low_ref[0, rows, :].astype(F32)).astype(BF16)
        pre = decay_base + dot(act, up_d)
        LD[rows, :] = shift_ref[rows, :] - jax.nn.sigmoid(pre) * 0.6065306597126334
        rate = jax.nn.sigmoid(rate_base + dot(low_ref[1, rows, :], up_r))
        key = proj_ref[rows, 4 * LANES : 5 * LANES].astype(F32)
        scaled = key * key_scale
        erase = scaled * lax.rsqrt(head_sum(scaled * scaled, ones) + norm_eps)
        AD[rows, :] = -erase
        BD[rows, :] = erase * rate
        KW[rows, :] = key * (1.0 + (rate - 1.0) * key_mix)

    t, s = row % HEAD, lane % HEAD
    strict = same_head & (t > s)
    causal = same_head & (t >= s)
    same32 = (t // 32) == (s // 32)
    eye = jnp.where(row == lane, 1.0, 0.0)
    offs = {
        b: same_head & ((t // (2 * b)) == (s // (2 * b))) & ((t // b) % 2 == 1) & ((s // b) % 2 == 0) for b in (1, 2, 4, 8, 16, 32)
    }
    low64 = lax.broadcasted_iota(jnp.int32, (BLOCK, LANES), 1) < HEAD
    row64 = lax.broadcasted_iota(jnp.int32, (BLOCK, LANES), 0)
    tri = jnp.where(
        lax.broadcasted_iota(jnp.int32, (BLOCK, BLOCK), 0) >= lax.broadcasted_iota(jnp.int32, (BLOCK, BLOCK), 1), 1.0, 0.0
    ).astype(BF16)

    def stacked(v):
        return jnp.concatenate([jnp.where(low64, v, 0.0), jnp.where(low64, 0.0, v)], axis=0)

    def pairs(a, q, b, k):
        left = jnp.concatenate([stacked(a), stacked(q)], axis=0)
        out = mm_nt_wide(left, jnp.concatenate([b, k, k, b], axis=0))
        head1 = lane >= HEAD
        first, second = out[:, :LANES], out[:, LANES:]
        pick = lambda f, g: jnp.where(head1, g, f)
        return (
            pick(first[:128], second[:128]), pick(second[:128], first[:128]),
            pick(first[128:], second[128:]), pick(second[128:], first[128:]),
        )

    def one_block(n):
        rows = pl.ds(pl.multiple_of(n * BLOCK, BLOCK), BLOCK)
        ld = LD[rows, :]
        lh, ll = halves(ld)
        lll = (ld - lh.astype(F32) - ll.astype(F32)).astype(BF16)
        L = dot(tri, lh) + dot(tri, ll) + dot(tri, lll)
        Lx = L - ld
        a, b, k = AD[rows, :], BD[rows, :], KW[rows, :]
        q = proj_ref[rows, 3 * LANES : 4 * LANES].astype(F32)
        v = proj_ref[rows, 5 * LANES : 6 * LANES].astype(F32)
        mid = jnp.where(row64 < 32, L[15:16, :], L[47:48, :])
        edge, end = L[31:32, :], L[63:64, :]
        back = jnp.exp(mid - L)
        near = pairs(a * jnp.exp(Lx - mid), q * jnp.exp(L - mid), b * back, k * back)
        back = jnp.exp(jnp.minimum(edge - L, 0.0))
        far = pairs(
            a * jnp.exp(jnp.minimum(Lx - edge, 0.0)), q * jnp.exp(jnp.minimum(L - edge, 0.0)), b * back, k * back
        )
        M, N, QB, QK = (
            jnp.where(mask, jnp.where(same32, f, g), 0.0) for mask, f, g in zip((strict, strict, causal, causal), near, far)
        )
        As, Vs = stacked(a * jnp.exp(Lx)), stacked(v)
        inv = eye + jnp.where(offs[1], M, 0.0)
        for w in (2, 4, 8, 16, 32):
            inv = inv + mm(mm(inv, jnp.where(offs[w], M, 0.0)), inv)
        both = mm_wide(inv, jnp.concatenate([As, mm(N, Vs)], axis=1))
        qboth = mm_wide(QB, both)
        qm = stacked(q * jnp.exp(L)) + qboth[:, :LANES]
        lo = qboth[:, LANES:] + mm(QK, Vs)
        ahead = jnp.exp(end - L)
        smT, leT = both[:, :LANES].T, both[:, LANES:].T
        gl = mm(jnp.concatenate([smT, leT], axis=0), stacked(b * ahead))
        G = gl[:128] + jnp.where(row == lane, jnp.exp(end), 0.0)
        H = gl[128:] + mm(Vs.T, stacked(k * ahead))
        GC[n, 0] = G
        GC[n, 1] = H
        QM[n] = qm
        LO[n] = lo[:BLOCK] + lo[BLOCK:]

    @pl.loop(0, 4)
    def _(i):
        for u in range(4):
            one_block(i * 4 + u)

    X[0:128, :] = eye
    X[128:256, :] = jnp.zeros((128, LANES), F32)

    @pl.loop(0, 4)
    def _(i):
        for u in range(4):
            n = i * 4 + u
            rows = pl.ds(pl.multiple_of(n * BLOCK, BLOCK), BLOCK)
            before = X[...]
            out = mm_nt_wide(QM[n], before)
            qp_ref[rows, :] = out[:BLOCK, :LANES] + out[BLOCK:, :LANES]
            loc_ref[rows, :] = out[:BLOCK, LANES:] + out[BLOCK:, LANES:] + LO[n]
            after = mm(before, GC[n, 0])
            X[0:128, :] = after[:128]
            X[128:256, :] = after[128:] + GC[n, 1]

    gh_ref[0:64, :] = (X[0:64, :] + X[64:128, :]).astype(BF16)
    gh_ref[64:128, :] = (X[128:192, :] + X[192:256, :]).astype(BF16)


def block_terms(proj, low, shift, up_d, up_r, par):
    vmem = pl.BlockSpec(memory_space=pltpu.VMEM)

    def kernel(*refs):
        block_kernel(None, *refs)

    return pl.pallas_call(
        kernel,
        name="block_terms",
        out_shape=(
            jax.ShapeDtypeStruct((1024, LANES), F32),
            jax.ShapeDtypeStruct((1024, LANES), F32),
            jax.ShapeDtypeStruct((128, LANES), BF16),
        ),
        in_specs=[vmem] * 6,
        out_specs=(vmem,) * 3,
        scratch_shapes=[
            pltpu.VMEM((1024, LANES), F32),
            pltpu.VMEM((1024, LANES), F32),
            pltpu.VMEM((1024, LANES), F32),
            pltpu.VMEM((1024, LANES), F32),
            pltpu.VMEM((16, 2, 128, LANES), F32),
            pltpu.VMEM((16, 128, LANES), F32),
            pltpu.VMEM((16, BLOCK, LANES), F32),
            pltpu.VMEM((256, LANES), F32),
        ],
        compiler_params=pltpu.CompilerParams(vmem_limit_bytes=48 << 20),
        cost_estimate=pl.CostEstimate(flops=4_000_000_000, bytes_accessed=4_000_000, transcendentals=2_000_000),
    )(proj, low, shift, up_d, up_r, par)


def finish_kernel(
    proj_ref, qp_ref, loc_ref, gh_ref, wout_ref, par_ref,
    out_ref,
    CH, HALO, S, Z, SB, RB, OB, S1, S2, R1, R2, S3, S4, R3, R4,
    g_send, g_recv, h_send, h_recv, b_send, b_recv, y_send, y_recv,
):
    z, y, x, c = here()

    def at(dz=0, dy=0, dc=0):
        return (lax.rem(z + dz, NZ), lax.rem(y + dy, NY), x, lax.rem(c + dc, 2))

    entered = enter([at(dz=d) for d in range(1, NZ)] + [at(dy=1), at(dy=3), at(dc=1)])
    mine = pl.ds(pl.multiple_of(y * LANES, LANES), LANES)
    entered()

    def chain_copy(d):
        return remote(gh_ref, CH.at[z], g_send.at[d], g_recv.at[z], at(dz=d))

    def halo_copy(k):
        return remote(proj_ref.at[1008:1024, k * LANES : k * LANES + LANES], HALO.at[k - 1], h_send.at[k - 1], h_recv.at[k - 1], at(dz=1))

    for d in range(1, NZ):

        @pl.when(z + d < NZ)
        def _():
            if d == 1:
                halo_copy(1).start()
                halo_copy(2).start()
            chain_copy(d).start()

    HALO_ZERO = jnp.zeros((16, LANES), BF16)

    @pl.when(z > 0)
    def _():
        halo_copy(1).wait_recv()
        halo_copy(2).wait_recv()

    @pl.when(z == 0)
    def _():
        HALO[0] = HALO_ZERO
        HALO[1] = HALO_ZERO

    tap0, tap1, tap2 = (par_ref[5 + k : 6 + k, mine] for k in range(3))
    before = HALO[0].astype(F32) * HALO[1].astype(F32)
    product = proj_ref[:, LANES : 2 * LANES].astype(F32) * proj_ref[:, 2 * LANES : 3 * LANES].astype(F32)
    whole = jnp.concatenate([before[8:16], product], axis=0)
    filtered = tap0 * whole[6:1030] + tap1 * whole[7:1031] + tap2 * product
    Z[:, 0:LANES] = (proj_ref[:, 0:LANES].astype(F32) * filtered).astype(BF16)

    low64 = lax.broadcasted_iota(jnp.int32, (HEAD, LANES), 1) < HEAD

    def stacked(v):
        zero = jnp.zeros_like(v)
        return jnp.concatenate([jnp.where(low64, v, zero), jnp.where(low64, zero, v)], axis=0)

    S[...] = jnp.zeros((HEAD, LANES), F32)
    for k in range(NZ - 1):

        @pl.when(z > k)
        def _():
            remote(gh_ref, CH.at[k], g_send.at[1], g_recv.at[k], at(dz=1)).wait_recv()
            high, low = halves(S[...])
            g = stacked(CH[k, 0:64, :])
            S[...] = dot(high, g) + dot(low, g) + CH[k, 64:128, :].astype(F32)

    lane = lax.broadcasted_iota(jnp.int32, (128, LANES), 1)
    row = lax.broadcasted_iota(jnp.int32, (128, LANES), 0)
    mean_of = jnp.where((row // HEAD) == (lane // HEAD), 1.0 / HEAD, 0.0).astype(BF16)
    start = stacked(S[...])
    start_h, start_l = halves(start)
    gain = par_ref[4:5, mine]

    @pl.loop(0, 4)
    def _(i):
        rows = pl.ds(pl.multiple_of(i * 256, 256), 256)
        qh, ql = halves(qp_ref[rows, :])
        readout = loc_ref[rows, :] + dot_nt(qh, start_h) + dot_nt(ql, start_h) + dot_nt(qh, start_l)
        centered = readout - head_sum(readout, mean_of)
        variance = head_sum(centered * centered, mean_of)
        Z[rows, LANES : 2 * LANES] = (centered * lax.rsqrt(variance + group_eps) * gain).astype(BF16)

    rel = (2, 1, 3, 0)
    other = at(dc=1)

    def to_other(k):
        return remote(SB.at[k], RB.at[k], b_send.at[k], b_recv.at[k], other)

    def part(k, core):
        rows = pl.ds(pl.multiple_of((lax.rem(y + rel[k], NY) * 2 + core) * 128, 128), 128)
        return dot_nt(Z[rows, :], wout_ref[...])

    for k in range(4):
        SB[k] = part(k, 1 - c).astype(BF16)
        to_other(k).start()
        OB[k] = part(k, c)

    def total(k, lo, hi):
        return OB[k, lo:hi, :] + RB[k, lo:hi, :].astype(F32)

    up, down = at(dy=1), at(dy=3)
    c1 = remote(S1, R1, y_send.at[0], y_recv.at[0], up)
    c2 = remote(S2, R2, y_send.at[1], y_recv.at[1], down)
    c3b = remote(S3.at[64:128], R3.at[64:128], y_send.at[2], y_recv.at[2], up)
    c4a = remote(S4.at[0:64], R4.at[0:64], y_send.at[3], y_recv.at[3], down)
    c3a = remote(S3.at[0:64], R3.at[0:64], y_send.at[4], y_recv.at[4], up)
    c4b = remote(S4.at[64:128], R4.at[64:128], y_send.at[5], y_recv.at[5], down)
    to_other(0).wait_recv()
    S1[...] = total(0, 0, 64).astype(BF16)
    S2[...] = total(0, 64, 128).astype(BF16)
    to_other(1).wait_recv()
    c1.start()
    c2.start()
    S3[64:128, :] = total(1, 64, 128).astype(BF16)
    to_other(2).wait_recv()
    S4[0:64, :] = total(2, 0, 64).astype(BF16)
    c3b.start()
    to_other(3).wait_recv()
    c4a.start()
    OB[3] = OB[3] + RB[3].astype(F32)
    c1.wait_recv()
    S3[0:64, :] = (total(1, 0, 64) + R1[...].astype(F32)).astype(BF16)
    c2.wait_recv()
    c3a.start()
    S4[64:128, :] = (total(2, 64, 128) + R2[...].astype(F32)).astype(BF16)
    c3b.wait_recv()
    c4b.start()
    c4a.wait_recv()
    c3a.wait_recv()
    c4b.wait_recv()
    out_ref[...] = (OB[3] + R3[...].astype(F32) + R4[...].astype(F32)).astype(BF16)
    for copy in (c1, c2, c3b, c4a, c3a, c4b):
        copy.wait_send()
    for k in range(4):
        to_other(k).wait_send()
    for d in range(1, NZ):

        @pl.when(z + d < NZ)
        def _():
            if d == 1:
                halo_copy(1).wait_send()
                halo_copy(2).wait_send()
            chain_copy(d).wait_send()


def finish(proj, qp, loc, gh, wout, par):
    vmem = pl.BlockSpec(memory_space=pltpu.VMEM)
    dma = pltpu.SemaphoreType.DMA
    block = lambda n: pltpu.VMEM((n, 2048), BF16)
    return pl.pallas_call(
        finish_kernel,
        name="finish",
        out_shape=jax.ShapeDtypeStruct((128, 2048), BF16),
        in_specs=[vmem] * 6,
        out_specs=vmem,
        scratch_shapes=[
            pltpu.VMEM((NZ, 128, LANES), BF16),
            pltpu.VMEM((2, 16, LANES), BF16),
            pltpu.VMEM((HEAD, LANES), F32),
            pltpu.VMEM((1024, 2 * LANES), BF16),
            pltpu.VMEM((4, 128, 2048), BF16),
            pltpu.VMEM((4, 128, 2048), BF16),
            pltpu.VMEM((4, 128, 2048), F32),
            block(64), block(64), block(64), block(64), block(128), block(128), block(128), block(128),
            dma((NZ,)), dma((NZ,)), dma((2,)), dma((2,)), dma((4,)), dma((4,)), dma((6,)), dma((6,)),
        ],
        compiler_params=pltpu.CompilerParams(collective_id=2, has_side_effects=True, vmem_limit_bytes=48 << 20),
        cost_estimate=pl.CostEstimate(flops=1_500_000_000, bytes_accessed=8_000_000, transcendentals=0),
    )(proj, qp, loc, gh, wout, par)


def body(
    tokens, norm_gain, w_conv_gate, w_conv_in, w_conv_value, conv_taps, w_receptance, w_key, w_value, w_decay_down,
    w_decay_up, decay_base, decay_shift, w_rate_down, w_rate_up, rate_base, key_scale, key_mix, group_gain,
    w_out_conv, w_out_state,
):
    first = lax.axis_index("tp") == 0
    low = jnp.where(first, w_decay_down, w_rate_down)
    pieces = [w.reshape(64, NY, LANES) for w in (w_conv_gate, w_conv_in, w_conv_value, w_receptance, w_key, w_value)]
    pieces.append(jnp.broadcast_to(low[:, None, :], (64, NY, LANES)))
    pieces += [w.T.reshape(64, NY, LANES) for w in (w_out_conv, w_out_state)]
    wp = jnp.concatenate(pieces, axis=2).transpose(1, 0, 2)
    par = jnp.concatenate(
        [jnp.stack([decay_base, rate_base, key_scale, key_mix, group_gain]), conv_taps], axis=0
    )
    proj, low, shift, wout = gather_and_project(tokens[0], norm_gain[None], wp, decay_shift[0])
    qp, loc, gh = block_terms(proj, low, shift, w_decay_up, w_rate_up, par)
    return finish(proj, qp, loc, gh, wout, par)[None]


def solution(mesh):
    split = Mesh(mesh.devices.reshape(NZ, NY, mesh.shape["fs"], mesh.shape["tp"]), AXES)
    placed = (
        P("fs", SP_TP, None), P(), P(SP, "tp"), P(SP, "tp"), P(SP, "tp"), P(None, "tp"), P(SP, "tp"), P(SP, "tp"),
        P(SP, "tp"), P(SP, None), P(None, "tp"), P("tp"), P("fs", SP, "tp"), P(SP, None), P(None, "tp"), P("tp"),
        P("tp"), P("tp"), P("tp"), P("tp", SP), P("tp", SP),
    )
    return jax.shard_map(
        body, mesh=split, in_specs=placed, out_specs=P("fs", SP_TP, None), check_vma=False
    )
```

profile of v0, /device:TPU:192, one launch (start us, length us, event | category | flops | bytes accessed | tf_op | source)
XLA Modules:
  0.0 136.6 jit_solution(14522432299850906895)
XLA Ops:
  0.0 0.0 copy-start
  0.0 0.8 broadcast_select_fusion
  0.8 0.8 concatenate.7.refs_5_.par_ref
  1.6 0.0 copy-done
  1.6 0.9 bitcast_dynamic-update-slice_fusion.6
  2.5 0.9 bitcast_dynamic-update-slice_fusion.5
  3.3 0.9 bitcast_dynamic-update-slice_fusion.4
  4.2 0.9 bitcast_dynamic-update-slice_fusion.3
  5.1 0.9 bitcast_dynamic-update-slice_fusion.2
  6.0 0.9 bitcast_dynamic-update-slice_fusion.1
  6.8 0.9 bitcast_dynamic-update-slice_fusion
  7.7 0.0 copy-start.1
  7.7 1.0 copy-done.1
  8.7 0.0 copy-start.2
  8.7 1.0 copy-done.2
  9.8 0.0 copy-start.5
  9.8 0.7 copy-done.5
  10.5 0.0 copy-start.3
  10.5 0.0 copy-start.4
  10.5 49.7 %gather_project.1 = (bf16[1024,768]{1,0:T(8,128)(2,1)S(1)}, bf16[2,1024,128]{2,1,0:T(8,128)(2,1)S(1)}, f32[1024,128]{1,0:T(8,128)S(1)}, bf16[2048,256]{1,0:T(8,128)(2,1)S(1)}) custom-call(bf16[128,2048]{1,0:T(8,128)(2,1)S(1)} %bitcast.54, f32[1,2048]{1,0:T(1,128)S(1)} %bitcast.56, bf16[4,64,1152]{2,1,0:T(8,128)(2,1)S(1)} %bitcast.53, f32[256,512]{1,0:T(8,128)S(1)} %bitcast.55), custom_call_target="tpu_custom_call" | custom-call | flops 4000000000 | bytes 16000000 | tf_op jit(solution)/shard_map/gather_project/pallas_call | solution.py:202
  60.2 0.0 copy-done.3
  60.2 0.0 copy-done.4
  60.2 34.7 %block_terms.1 = (f32[1024,128]{1,0:T(8,128)S(1)}, f32[1024,128]{1,0:T(8,128)S(1)}, bf16[128,128]{1,0:T(8,128)(2,1)S(1)}) custom-call(bf16[1024,768]{1,0:T(8,128)(2,1)S(1)} %get-tuple-element.12.refs_0_.proj_ref, bf16[2,1024,128]{2,1,0:T(8,128)(2,1)S(1)} %get-tuple-element.13.refs_1_, f32[1024,128]{1,0:T(8,128)S(1)} %get-tuple-element.14.refs_2_, ...), custom_call_target="tpu_custom_call" | custom-call | flops 4000000000 | bytes 4000000 | tf_op jit(solution)/shard_map/block_terms/pallas_call | solution.py:391
  94.9 40.8 %finish.1 = bf16[128,2048]{1,0:T(8,128)(2,1)S(1)} custom-call(bf16[1024,768]{1,0:T(8,128)(2,1)S(1)} %get-tuple-element.12.refs_0_.proj_ref, f32[1024,128]{1,0:T(8,128)S(1)} %get-tuple-element.15.qp_ref, f32[1024,128]{1,0:T(8,128)S(1)} %get-tuple-element.16.loc_ref, bf16[128,128]{1,0:T(8,128)(2,1)S(1)} %get-tuple-element.17.gh_ref, ...), custom_call_target="tpu_custom_call" | custom-call | flops 1500000000 | bytes 8000000 | tf_op jit(solution)/shard_map/finish/pallas_call | solution.py:564
  135.8 0.8 copy.55
  (2 shorter events, 0.0 us)
Async XLA Ops:
  0.0 1.6 %copy-start = (bf16[64,512]{1,0:T(8,128)(2,1)S(1)}, bf16[64,512]{1,0:T(8,128)(2,1)}, u32[]{:S(2)}) copy-start(bf16[64,512]{1,0:T(8,128)(2,1)} %param.23) | copy-start | bytes 196612
  7.7 1.0 copy-start.1
  8.7 1.0 copy-start.2
  9.8 0.7 copy-start.5
  10.5 49.7 %copy-start.3 = (bf16[128,512]{1,0:T(8,128)(2,1)S(1)}, bf16[128,512]{1,0:T(8,128)(2,1)}, u32[]{:S(2)}) copy-start(bf16[128,512]{1,0:T(8,128)(2,1)} %refs_3_.1) | copy-start | bytes 393220
  10.5 49.7 %copy-start.4 = (bf16[128,512]{1,0:T(8,128)(2,1)S(1)}, bf16[128,512]{1,0:T(8,128)(2,1)}, u32[]{:S(2)}) copy-start(bf16[128,512]{1,0:T(8,128)(2,1)} %refs_4_.1) | copy-start | bytes 393220
where the time goes:
time: 137 us
  Pallas kernels  125 us (91%)
  local copies, waits for them, and re-layouts  10.5 us (8%)
    pallas_call x1, Pallas kernels, gather_and_project(): pl.pallas_call(gather_kernel, name='gather_project', out_shape=(jax.Shape...  49.7 us
    pallas_call x1, Pallas kernels, finish(): pl.pallas_call(finish_kernel, name='finish', out_shape=jax.ShapeDtypeStru...  40.8 us
    pallas_call x1, Pallas kernels, block_terms(): pl.pallas_call(kernel, name='block_terms', out_shape=(jax.ShapeDtypeStruc...  34.7 us
    unnamed x21, local copies, waits for them, and re-layouts  8.81 us

commit v1 on v0

--- a/solution.py
+++ b/solution.py
@@ -164,25 +164,16 @@
     for copy in crossed:
         copy.wait_recv()
 
-    def rows_of(i):
-        return T[i].reshape(256, 2048)
-
-    @pl.loop(0, NY)
-    def _(i):
-        w = W[:, :, :, :, 6 * LANES : 7 * LANES].reshape(2048, LANES)
-        out = jnp.dot(rows_of(i), w, preferred_element_type=F32)
-        LOW[c, pl.ds(pl.multiple_of(i * 256, 256), 256), :] = out.astype(BF16)
-
+    def project(first, count):
+        rows = T[...].reshape(1024, 2048)
+        w = W[:, :, :, :, first * LANES : (first + count) * LANES].reshape(2048, count * LANES)
+        return jnp.dot(rows, w, preferred_element_type=F32).astype(BF16)
+
+    LOW[c] = project(6, 1)
     low_copy = remote(LOW.at[c], LOW.at[c], l_send.at[0], l_recv.at[0], other)
     low_copy.start()
-
-    @pl.loop(0, NY)
-    def _(i):
-        rows = pl.ds(pl.multiple_of(i * 256, 256), 256)
-        for n in range(3):
-            w = W[:, :, :, :, n * 256 : n * 256 + 256].reshape(2048, 256)
-            out = jnp.dot(rows_of(i), w, preferred_element_type=F32)
-            proj_ref[rows, n * 256 : n * 256 + 256] = out.astype(BF16)
+    for n in (0, 2, 4):
+        proj_ref[:, n * LANES : (n + 2) * LANES] = project(n, 2)
 
     wout_ref[...] = W[:, :, :, :, 7 * LANES :].reshape(2048, 256)
     for d in (1, 2, 3):
@@ -244,16 +235,12 @@
     return out[:, :LANES] + out[:, LANES:]
 
 
-def mm_wide(a, b):
-    ah, al = halves(a)
-    bh, bl = halves(b)
-    return dot(jnp.concatenate([ah, al], axis=1), jnp.concatenate([bh, bh], axis=0)) + dot(ah, bl)
-
-
-def mm_nt_wide(a, b):
-    ah, al = halves(a)
-    bh, bl = halves(b)
-    return dot_nt(jnp.concatenate([ah, al], axis=1), jnp.concatenate([bh, bh], axis=1)) + dot_nt(ah, bl)
+def mm1(a, b):
+    return dot(a.astype(BF16), b.astype(BF16))
+
+
+def nt1(a, b):
+    return dot_nt(a.astype(BF16), b.astype(BF16))
 
 
 def head_sum(values, ones):
@@ -309,7 +296,7 @@
 
     def pairs(a, q, b, k):
         left = jnp.concatenate([stacked(a), stacked(q)], axis=0)
-        out = mm_nt_wide(left, jnp.concatenate([b, k, k, b], axis=0))
+        out = nt1(left, jnp.concatenate([b, k, k, b], axis=0))
         head1 = lane >= HEAD
         first, second = out[:, :LANES], out[:, LANES:]
         pick = lambda f, g: jnp.where(head1, g, f)
@@ -319,7 +306,7 @@
         )
 
     def one_block(n):
-        rows = pl.ds(pl.multiple_of(n * BLOCK, BLOCK), BLOCK)
+        rows = pl.ds(n * BLOCK, BLOCK)
         ld = LD[rows, :]
         lh, ll = halves(ld)
         lll = (ld - lh.astype(F32) - ll.astype(F32)).astype(BF16)
@@ -332,35 +319,49 @@
         edge, end = L[31:32, :], L[63:64, :]
         back = jnp.exp(mid - L)
         near = pairs(a * jnp.exp(Lx - mid), q * jnp.exp(L - mid), b * back, k * back)
+        yield
         back = jnp.exp(jnp.minimum(edge - L, 0.0))
         far = pairs(
             a * jnp.exp(jnp.minimum(Lx - edge, 0.0)), q * jnp.exp(jnp.minimum(L - edge, 0.0)), b * back, k * back
         )
+        yield
         M, N, QB, QK = (
             jnp.where(mask, jnp.where(same32, f, g), 0.0) for mask, f, g in zip((strict, strict, causal, causal), near, far)
         )
         As, Vs = stacked(a * jnp.exp(Lx)), stacked(v)
+        NV = mm1(N, Vs)
+        yield
+        lo = mm1(QK, Vs)
+        yield
         inv = eye + jnp.where(offs[1], M, 0.0)
         for w in (2, 4, 8, 16, 32):
-            inv = inv + mm(mm(inv, jnp.where(offs[w], M, 0.0)), inv)
-        both = mm_wide(inv, jnp.concatenate([As, mm(N, Vs)], axis=1))
-        qboth = mm_wide(QB, both)
+            part = mm(inv, jnp.where(offs[w], M, 0.0))
+            yield
+            inv = inv + mm(part, inv)
+            yield
+        both = mm1(inv, jnp.concatenate([As, NV], axis=1))
+        yield
+        qboth = mm1(QB, both)
+        yield
         qm = stacked(q * jnp.exp(L)) + qboth[:, :LANES]
-        lo = qboth[:, LANES:] + mm(QK, Vs)
+        lo = qboth[:, LANES:] + lo
+        QM[n] = qm
+        LO[n] = lo[:BLOCK] + lo[BLOCK:]
         ahead = jnp.exp(end - L)
         smT, leT = both[:, :LANES].T, both[:, LANES:].T
-        gl = mm(jnp.concatenate([smT, leT], axis=0), stacked(b * ahead))
+        gl = mm1(jnp.concatenate([smT, leT], axis=0), stacked(b * ahead))
+        yield
         G = gl[:128] + jnp.where(row == lane, jnp.exp(end), 0.0)
-        H = gl[128:] + mm(Vs.T, stacked(k * ahead))
+        H = gl[128:] + mm1(Vs.T, stacked(k * ahead))
         GC[n, 0] = G
         GC[n, 1] = H
-        QM[n] = qm
-        LO[n] = lo[:BLOCK] + lo[BLOCK:]
-
-    @pl.loop(0, 4)
-    def _(i):
-        for u in range(4):
-            one_block(i * 4 + u)
+
+    def in_step(blocks):
+        blocks = list(blocks)
+        while blocks:
+            blocks = [b for b in blocks if next(b, True) is None]
+
+    in_step(one_block(u) for u in range(16))
 
     X[0:128, :] = eye
     X[128:256, :] = jnp.zeros((128, LANES), F32)
@@ -371,7 +372,7 @@
             n = i * 4 + u
             rows = pl.ds(pl.multiple_of(n * BLOCK, BLOCK), BLOCK)
             before = X[...]
-            out = mm_nt_wide(QM[n], before)
+            out = nt1(QM[n], before)
             qp_ref[rows, :] = out[:BLOCK, :LANES] + out[BLOCK:, :LANES]
             loc_ref[rows, :] = out[:BLOCK, LANES:] + out[BLOCK:, LANES:] + LO[n]
             after = mm(before, GC[n, 0])

time: 137 us -> 116 us (0.85)
  Pallas kernels: 125 us -> 104 us
    pallas_call x1, Pallas kernels: 34.7 us -> 12.3 us  [block_terms(): pl.pallas_call(kernel, name='block_terms', out_shape=(jax.ShapeDtypeStruc...]
where the time goes in v1:
time: 116 us; the launch traced here: 115 us
  Pallas kernels  104 us (90%)
  local copies, waits for them, and re-layouts  10.5 us (9%)
    pallas_call x1, Pallas kernels, gather_and_project(): pl.pallas_call(gather_kernel, name='gather_project', out_shape=(jax.Shape...  50.9 us
    pallas_call x1, Pallas kernels, finish(): pl.pallas_call(finish_kernel, name='finish', out_shape=jax.ShapeDtypeStru...  40.8 us
    pallas_call x1, Pallas kernels, block_terms(): pl.pallas_call(kernel, name='block_terms', out_shape=(jax.ShapeDtypeStruc...  12.3 us
    unnamed x21, local copies, waits for them, and re-layouts  8.81 us

profile of v1, /device:TPU:192, one launch (start us, length us, event | category | flops | bytes accessed | tf_op | source)
XLA Modules:
  0.0 115.4 jit_solution(12251906171896047954)
XLA Ops:
  0.0 0.0 copy-start
  0.0 0.8 broadcast_select_fusion
  0.8 0.8 concatenate.7.refs_5_.par_ref
  1.6 0.0 copy-done
  1.6 0.9 bitcast_dynamic-update-slice_fusion.6
  2.5 0.9 bitcast_dynamic-update-slice_fusion.5
  3.3 0.9 bitcast_dynamic-update-slice_fusion.4
  4.2 0.9 bitcast_dynamic-update-slice_fusion.3
  5.1 0.9 bitcast_dynamic-update-slice_fusion.2
  6.0 0.9 bitcast_dynamic-update-slice_fusion.1
  6.8 0.9 bitcast_dynamic-update-slice_fusion
  7.7 0.0 copy-start.1
  7.7 1.0 copy-done.1
  8.7 0.0 copy-start.2
  8.7 1.0 copy-done.2
  9.8 0.0 copy-start.5
  9.8 0.7 copy-done.5
  10.5 0.0 copy-start.3
  10.5 0.0 copy-start.4
  10.5 50.9 %gather_project.1 = (bf16[1024,768]{1,0:T(8,128)(2,1)S(1)}, bf16[2,1024,128]{2,1,0:T(8,128)(2,1)S(1)}, f32[1024,128]{1,0:T(8,128)S(1)}, bf16[2048,256]{1,0:T(8,128)(2,1)S(1)}) custom-call(bf16[128,2048]{1,0:T(8,128)(2,1)S(1)} %bitcast.54, f32[1,2048]{1,0:T(1,128)S(1)} %bitcast.56, bf16[4,64,1152]{2,1,0:T(8,128)(2,1)S(1)} %bitcast.53, f32[256,512]{1,0:T(8,128)S(1)} %bitcast.55), custom_call_target="tpu_custom_call" | custom-call | flops 4000000000 | bytes 16000000 | tf_op jit(solution)/shard_map/gather_project/pallas_call | solution.py:193
  61.4 0.0 copy-done.3
  61.4 0.0 copy-done.4
  61.4 12.3 %block_terms.1 = (f32[1024,128]{1,0:T(8,128)S(1)}, f32[1024,128]{1,0:T(8,128)S(1)}, bf16[128,128]{1,0:T(8,128)(2,1)S(1)}) custom-call(bf16[1024,768]{1,0:T(8,128)(2,1)S(1)} %get-tuple-element.12.refs_0_.proj_ref, bf16[2,1024,128]{2,1,0:T(8,128)(2,1)S(1)} %get-tuple-element.13.refs_1_, f32[1024,128]{1,0:T(8,128)S(1)} %get-tuple-element.14.refs_2_, ...), custom_call_target="tpu_custom_call" | custom-call | flops 4000000000 | bytes 4000000 | tf_op jit(solution)/shard_map/block_terms/pallas_call | solution.py:392
  73.8 40.8 %finish.1 = bf16[128,2048]{1,0:T(8,128)(2,1)S(1)} custom-call(bf16[1024,768]{1,0:T(8,128)(2,1)S(1)} %get-tuple-element.12.refs_0_.proj_ref, f32[1024,128]{1,0:T(8,128)S(1)} %get-tuple-element.15.qp_ref, f32[1024,128]{1,0:T(8,128)S(1)} %get-tuple-element.16.loc_ref, bf16[128,128]{1,0:T(8,128)(2,1)S(1)} %get-tuple-element.17.gh_ref, ...), custom_call_target="tpu_custom_call" | custom-call | flops 1500000000 | bytes 8000000 | tf_op jit(solution)/shard_map/finish/pallas_call | solution.py:565
  114.6 0.8 copy.55
  (2 shorter events, 0.0 us)
Async XLA Ops:
  0.0 1.6 %copy-start = (bf16[64,512]{1,0:T(8,128)(2,1)S(1)}, bf16[64,512]{1,0:T(8,128)(2,1)}, u32[]{:S(2)}) copy-start(bf16[64,512]{1,0:T(8,128)(2,1)} %param.23) | copy-start | bytes 196612
  7.7 1.0 copy-start.1
  8.7 1.0 copy-start.2
  9.8 0.7 copy-start.5
  10.5 50.9 %copy-start.3 = (bf16[128,512]{1,0:T(8,128)(2,1)S(1)}, bf16[128,512]{1,0:T(8,128)(2,1)}, u32[]{:S(2)}) copy-start(bf16[128,512]{1,0:T(8,128)(2,1)} %refs_3_.1) | copy-start | bytes 393220
  10.5 50.9 %copy-start.4 = (bf16[128,512]{1,0:T(8,128)(2,1)S(1)}, bf16[128,512]{1,0:T(8,128)(2,1)}, u32[]{:S(2)}) copy-start(bf16[128,512]{1,0:T(8,128)(2,1)} %refs_4_.1) | copy-start | bytes 393220
